TPU v7x, 32 devices: a whole 2x2x4 slice. The times are simulated.
32 devices in a mesh: grp: 2 (over y), ra: 4 (over z), cb: 4 (over x, core).
Axes of the slice: x: 2, y: 2, z: 4, core: 2. Of those that a mesh axis runs over, the one named last changes fastest.
Arguments:
- stream: bfloat16 [256, 4096], P('grp', 'ra'), parts along dimension 0, may hold values from -180 to 180
- w_gate: float32 [2, 4096, 11264], P(None, 'ra', 'cb'), may hold values from -0.09375 to 0.09375
- w_up: float32 [2, 4096, 11264], P(None, 'ra', 'cb'), may hold values from -0.09375 to 0.09375
- w_down: float32 [2, 11264, 4096], P(None, 'cb', 'ra'), may hold values from -0.0546875 to 0.0546875
- gate_scale: float32 [2, 11264], P(None, 'cb'), may hold values from 0.5 to 2
- up_scale: float32 [2, 11264], P(None, 'cb'), may hold values from 0.5 to 2
- down_scale: float32 [2, 4096], P(None, 'ra'), may hold values from 0.5 to 2
- pre_gain: float32 [2, 4096], P(None, 'ra'), may hold values from 0.1 to 1.9
- out_gain: float32 [4096], P('ra'), may hold values from 0.1 to 1.9
Outputs:
- normed: bfloat16 [256, 4096], P('grp', 'ra'), parts along dimension 0
There are 2 independent parts, one for each index of `grp`. A program takes and returns all parts, laid end to end along the dimension named above; an argument that names none is the same for every part. Nothing has to cross between parts.
All inputs are finite; a program needn't handle non-finite values.
Results may differ from a plain program's by a relative error of at most 0.018.
Values may be sent and summed in bfloat16 or wider, within the bound.
A program may use at most 192 MiB of HBM per device.

v0:
```python
import jax
import jax.numpy as jnp
from jax import lax
from jax.sharding import PartitionSpec as P

D = 4096
LAYERS = 2


def local(stream, w_gate, w_up, w_down, gate_scale, up_scale, down_scale, pre_gain, out_gain):
    current = stream
    tokens = stream.shape[0]
    share = tokens // lax.axis_size("ra")
    for layer in range(LAYERS):
        xvals = current.astype(jnp.float32)
        squares = jnp.sum(xvals * xvals, axis=1)
        scaled = (xvals * pre_gain[layer]).astype(jnp.bfloat16)
        gate_part = jnp.dot(
            scaled, w_gate[layer].astype(jnp.bfloat16), preferred_element_type=jnp.float32
        )
        up_part = jnp.dot(
            scaled, w_up[layer].astype(jnp.bfloat16), preferred_element_type=jnp.float32
        )
        down_local = w_down[layer].astype(jnp.bfloat16)
        total = lax.psum(squares, "ra")
        operands = (gate_part, up_part)
        summed = (
            lax.psum_scatter(operands[0], "ra", scatter_dimension=0, tiled=True),
            lax.psum_scatter(operands[1], "ra", scatter_dimension=0, tiled=True),
        )
        own_rows = lax.dynamic_slice_in_dim(total, lax.axis_index("ra") * share, share)
        rinv = lax.rsqrt(own_rows / D + 1e-06)[:, None]
        gate = summed[0] * rinv * gate_scale[layer]
        upper = summed[1] * rinv * up_scale[layer]
        hidden = (jax.nn.silu(gate) * upper).astype(jnp.bfloat16)
        terms = jnp.dot(
            lax.all_gather(hidden, "ra", axis=0, tiled=True),
            down_local,
            preferred_element_type=jnp.float32,
        )
        branch = lax.psum(terms.astype(jnp.bfloat16), "cb").astype(jnp.float32) * down_scale[layer]
        current = (0.5 * xvals + branch).astype(jnp.bfloat16)
    xvals = current.astype(jnp.float32)
    final_sum = lax.psum(jnp.sum(xvals * xvals, axis=1), "ra")
    rinv = lax.rsqrt(final_sum / D + 1e-06)[:, None]
    return (xvals * rinv * out_gain).astype(jnp.bfloat16)


def solution(mesh):
    placed = (
        P("grp", "ra"),
        P(None, "ra", "cb"),
        P(None, "ra", "cb"),
        P(None, "cb", "ra"),
        P(None, "cb"),
        P(None, "cb"),
        P(None, "ra"),
        P(None, "ra"),
        P("ra"),
    )
    return jax.shard_map(
        local, mesh=mesh, in_specs=placed, out_specs=P("grp", "ra"), check_vma=False
    )
```

profile of v0, /device:TPU:0, one launch (start us, length us, event | category | flops | bytes accessed | tf_op | source)
XLA Modules:
  0.0 296.9 jit_solution(10310652706290276706)
XLA Ops:
  6.5 0.8 fusion.24
  7.3 0.0 copy-start.2
  7.3 8.6 %convert.12 = bf16[2,1024,2816]{2,1,0:T(8,128)(2,1)S(1)} convert(f32[2,1024,2816]{2,1,0:T(8,128)} %param.10) | non-fusion elementwise | flops 5767168 | bytes 34603008 | tf_op jit(solution)/shard_map/convert.5
  15.9 0.0 copy-start.1
  15.9 4.2 %copy-done.1 = bf16[2,1024,2816]{2,1,0:T(8,128)(2,1)} copy-done((bf16[2,1024,2816]{2,1,0:T(8,128)(2,1)}, bf16[2,1024,2816]{2,1,0:T(8,128)(2,1)S(1)}, u32[]{:S(2)}) %copy-start.1) | copy-done | bytes 11534360
  20.1 2.0 fusion.5
  22.2 0.0 reduce-scatter.5.cloned.1.call-update
  22.2 0.0 reduce-scatter.7.cloned.1.call-start
  22.2 8.6 %convert.13 = bf16[2,1024,2816]{2,1,0:T(8,128)(2,1)S(1)} convert(f32[2,1024,2816]{2,1,0:T(8,128)} %param.11) | non-fusion elementwise | flops 5767168 | bytes 34603008 | tf_op jit(solution)/shard_map/convert.4
  30.8 4.2 %copy-done = bf16[2,1024,2816]{2,1,0:T(8,128)(2,1)} copy-done((bf16[2,1024,2816]{2,1,0:T(8,128)(2,1)}, bf16[2,1024,2816]{2,1,0:T(8,128)(2,1)S(1)}, u32[]{:S(2)}) %copy-start) | copy-done | bytes 11534360
  35.0 2.1 fusion.4
  37.1 0.0 reduce-scatter.7.cloned.1.call-update
  37.1 0.0 all-reduce.3.cloned.1.call-start
  37.2 0.0 copy-start.3
  37.2 0.0 copy-start.4
  37.2 12.6 %convert.14 = bf16[2,2816,1024]{2,1,0:T(8,128)(2,1)} convert(f32[2,2816,1024]{2,1,0:T(8,128)} %param.12) | non-fusion elementwise | flops 5767168 | bytes 34603008 | tf_op jit(solution)/shard_map/convert.3
  49.8 0.1 fusion.14
  50.0 13.6 %psum.35 = f32[128]{0:T(128)S(1)} all-reduce(f32[128]{0:T(128)S(1)} %fusion.14), channel_id=1, replica_groups=mesh['grp'=2,'ra'=4,'cb'=4] {'ra'}, use_global_device_ids=true, to_apply=%region_2.0 | all-reduce | flops 128 | bytes 1024 | tf_op jit(solution)/shard_map/psum | solution.py:25
  63.6 0.1 add_rsqrt_fusion.2
  63.7 0.1 slice_reduce_fusion
  63.8 0.0 reduce-scatter.5.cloned.1.call-done
  63.8 29.2 %reduce-scatter.7.cloned.1.call-done = f32[32,2816]{1,0:T(8,128)} async-done(((f32[128,2816]{1,0:T(8,128)}), f32[32,2816]{1,0:T(8,128)}) %reduce-scatter.7.cloned.1.call-update) | async-done | bytes 360464 | tf_op jit(solution)/shard_map/reduce_scatter | solution.py:29
  93.0 1.3 multiply_convert_fusion.1
  94.3 17.2 %all_gather.6 = bf16[128,2816]{1,0:T(8,128)(2,1)S(1)} all-gather(bf16[32,2816]{1,0:T(8,128)(2,1)S(1)} %multiply_convert_fusion.1), channel_id=1, replica_groups=mesh['grp'=2,'ra'=4,'cb'=4] {'ra'}, dimensions={0}, use_global_device_ids=true | all-gather | bytes 901120 | tf_op jit(solution)/shard_map/all_gather | solution.py:37
  111.5 4.3 %fusion.6 = bf16[128,1024]{1,0:T(8,128)(2,1)} fusion(bf16[128,2816]{1,0:T(8,128)(2,1)S(1)} %all_gather.6, bf16[2,2816,1024]{2,1,0:T(8,128)(2,1)} %convert.14), kind=kOutput, calls=%fused_computation.12 | convolution fusion | flops 738328576 | bytes 6750208 | tf_op jit(solution)/shard_map/dot_general | solution.py:36
  115.8 0.0 all-reduce.3.cloned.1.call-update
  115.8 0.0 reduce-scatter.9.cloned.1.call-start
  115.9 31.3 %all-reduce.3.cloned.1.call-done = bf16[128,1024]{1,0:T(8,128)(2,1)} async-done(((bf16[128,1024]{1,0:T(8,128)(2,1)}), bf16[128,1024]{1,0:T(8,128)(2,1)}) %all-reduce.3.cloned.1.call-update) | async-done | bytes 262160 | tf_op jit(solution)/shard_map/psum | solution.py:41
  147.2 1.2 fusion.18
  148.4 4.7 %fusion.2 = f32[128,2816]{1,0:T(8,128)} fusion(bf16[2,1024,2816]{2,1,0:T(8,128)(2,1)} %copy-done.1, bf16[128,1024]{1,0:T(8,128)(2,1)S(1)} %get-tuple-element.10, f32[1024]{0:T(1024)S(1)} %bitcast.31), kind=kOutput, calls=%fused_computation.5 | convolution fusion | flops 738590720 | bytes 7475200 | tf_op jit(solution)/shard_map/dot_general | solution.py:18
  153.1 0.0 reduce-scatter.9.cloned.1.call-update
  153.1 0.0 reduce-scatter.11.cloned.1.call-start
  153.1 4.7 %fusion.1 = f32[128,2816]{1,0:T(8,128)} fusion(bf16[2,1024,2816]{2,1,0:T(8,128)(2,1)} %copy-done, bf16[128,1024]{1,0:T(8,128)(2,1)S(1)} %get-tuple-element.10, f32[1024]{0:T(1024)S(1)} %bitcast.32), kind=kOutput, calls=%fused_computation.3 | convolution fusion | flops 738590720 | bytes 7475200 | tf_op jit(solution)/shard_map/dot_general | solution.py:21
  157.8 0.0 reduce-scatter.11.cloned.1.call-update
  157.8 0.0 copy-start.6
  157.9 0.0 all-reduce.5.cloned.1.call-start
  157.9 12.3 %psum.37 = f32[128]{0:T(128)S(1)} all-reduce(f32[128]{0:T(128)S(1)} %get-tuple-element.9), channel_id=1, replica_groups=mesh['grp'=2,'ra'=4,'cb'=4] {'ra'}, use_global_device_ids=true, to_apply=%region_7.8 | all-reduce | flops 128 | bytes 1024 | tf_op jit(solution)/shard_map/psum | solution.py:25
  170.2 0.1 add_rsqrt_fusion.1
  170.3 16.5 %reduce-scatter.9.cloned.1.call-done = f32[32,2816]{1,0:T(8,128)} async-done(((f32[128,2816]{1,0:T(8,128)}), f32[32,2816]{1,0:T(8,128)}) %reduce-scatter.9.cloned.1.call-update) | async-done | bytes 360464 | tf_op jit(solution)/shard_map/reduce_scatter | solution.py:28
  186.8 34.4 %reduce-scatter.11.cloned.1.call-done = f32[32,2816]{1,0:T(8,128)} async-done(((f32[128,2816]{1,0:T(8,128)}), f32[32,2816]{1,0:T(8,128)}) %reduce-scatter.11.cloned.1.call-update) | async-done | bytes 360464 | tf_op jit(solution)/shard_map/reduce_scatter | solution.py:29
  221.2 1.3 multiply_convert_fusion
  222.5 17.2 %all_gather.7 = bf16[128,2816]{1,0:T(8,128)(2,1)S(1)} all-gather(bf16[32,2816]{1,0:T(8,128)(2,1)S(1)} %multiply_convert_fusion), channel_id=1, replica_groups=mesh['grp'=2,'ra'=4,'cb'=4] {'ra'}, dimensions={0}, use_global_device_ids=true | all-gather | bytes 901120 | tf_op jit(solution)/shard_map/all_gather | solution.py:37
  239.6 4.3 %fusion.7 = bf16[128,1024]{1,0:T(8,128)(2,1)} fusion(bf16[128,2816]{1,0:T(8,128)(2,1)S(1)} %all_gather.7, bf16[2,2816,1024]{2,1,0:T(8,128)(2,1)} %convert.14), kind=kOutput, calls=%fused_computation.13 | convolution fusion | flops 738328576 | bytes 6750208 | tf_op jit(solution)/shard_map/dot_general | solution.py:36
  244.0 0.0 all-reduce.5.cloned.1.call-update
  244.0 31.5 %all-reduce.5.cloned.1.call-done = bf16[128,1024]{1,0:T(8,128)(2,1)} async-done(((bf16[128,1024]{1,0:T(8,128)(2,1)}), bf16[128,1024]{1,0:T(8,128)(2,1)}) %all-reduce.5.cloned.1.call-update) | async-done | bytes 262160 | tf_op jit(solution)/shard_map/psum | solution.py:41
  275.5 1.2 fusion.8
  276.6 11.7 %psum.39 = f32[128]{0:T(128)S(1)} all-reduce(f32[128]{0:T(128)S(1)} %fusion.8), channel_id=1, replica_groups=mesh['grp'=2,'ra'=4,'cb'=4] {'ra'}, use_global_device_ids=true, to_apply=%region_11.12 | all-reduce | flops 128 | bytes 1024 | tf_op jit(solution)/shard_map/psum | solution.py:44
  288.3 1.8 fusion.10
  (10 shorter events, 0.0 us)
Async XLA Ops:
  6.5 57.3 %reduce-scatter.5.cloned.1.call-start = ((), (), s32[]{:S(2)}) async-start(), calls=%async_computation.4 | async-start | bytes 1802240 | tf_op jit(solution)/shard_map/reduce_scatter | solution.py:28
  7.3 12.8 %copy-start.2 = (bf16[128,1024]{1,0:T(8,128)(2,1)S(1)}, bf16[128,1024]{1,0:T(8,128)(2,1)}, u32[]{:S(2)}) copy-start(bf16[128,1024]{1,0:T(8,128)(2,1)} %param.9) | copy-start | bytes 786436
  15.9 4.2 %copy-start.1 = (bf16[2,1024,2816]{2,1,0:T(8,128)(2,1)}, bf16[2,1024,2816]{2,1,0:T(8,128)(2,1)S(1)}, u32[]{:S(2)}) copy-start(bf16[2,1024,2816]{2,1,0:T(8,128)(2,1)S(1)} %convert.12) | copy-start | bytes 34603012
  22.2 70.9 %reduce-scatter.7.cloned.1.call-start = ((), (), s32[]{:S(2)}) async-start(), calls=%async_computation.5 | async-start | bytes 1802240 | tf_op jit(solution)/shard_map/reduce_scatter | solution.py:29
  30.8 4.2 %copy-start = (bf16[2,1024,2816]{2,1,0:T(8,128)(2,1)}, bf16[2,1024,2816]{2,1,0:T(8,128)(2,1)S(1)}, u32[]{:S(2)}) copy-start(bf16[2,1024,2816]{2,1,0:T(8,128)(2,1)S(1)} %convert.13) | copy-start | bytes 34603012
  37.1 110.1 %all-reduce.3.cloned.1.call-start = ((), (), s32[]{:S(2)}) async-start(), calls=%async_computation.6 | async-start | bytes 524288 | tf_op jit(solution)/shard_map/psum | solution.py:41
  37.2 26.5 %copy-start.3 = (f32[2,2816]{1,0:T(2,128)S(1)}, f32[2,2816]{1,0:T(2,128)}, u32[]{:S(2)}) copy-start(f32[2,2816]{1,0:T(2,128)} %param.14) | copy-start | bytes 67588
  37.2 26.5 %copy-start.4 = (f32[2,2816]{1,0:T(2,128)S(1)}, f32[2,2816]{1,0:T(2,128)}, u32[]{:S(2)}) copy-start(f32[2,2816]{1,0:T(2,128)} %param.13) | copy-start | bytes 67588
  49.8 66.1 %copy-start.5 = (f32[2,1024]{1,0:T(2,128)S(1)}, f32[2,1024]{1,0:T(2,128)}, u32[]{:S(2)}) copy-start(f32[2,1024]{1,0:T(2,128)} %param.15) | copy-start | bytes 24580
  115.8 71.0 %reduce-scatter.9.cloned.1.call-start = ((), (), s32[]{:S(2)}) async-start(), calls=%async_computation.7 | async-start | bytes 1802240 | tf_op jit(solution)/shard_map/reduce_scatter | solution.py:28
  153.1 68.1 %reduce-scatter.11.cloned.1.call-start = ((), (), s32[]{:S(2)}) async-start(), calls=%async_computation.8 | async-start | bytes 1802240 | tf_op jit(solution)/shard_map/reduce_scatter | solution.py:29
  157.8 130.5 %copy-start.6 = (f32[1024]{0:T(1024)S(1)}, f32[1024]{0:T(1024)}, u32[]{:S(2)}) copy-start(f32[1024]{0:T(1024)} %param.17) | copy-start | bytes 12292
  157.9 117.6 %all-reduce.5.cloned.1.call-start = ((), (), s32[]{:S(2)}) async-start(), calls=%async_computation.9 | async-start | bytes 524288 | tf_op jit(solution)/shard_map/psum | solution.py:41
Sparse Core Ops, SparseCore 0:
  22.3 36.0 reduce-scatter.4
  60.8 32.2 reduce-scatter.6
  116.0 31.2 all-reduce.2
  153.2 33.5 reduce-scatter.8
  189.0 32.1 reduce-scatter.10
  244.1 31.3 all-reduce.4
where the time goes:
time: 298 us; the launch traced here: 297 us
  waiting for transfers between devices  143 us (48%)
  blocking collectives  71.9 us (24%)
  other arithmetic  36.8 us (12%)
  matrix products  22 us (7%)
  between operations  13.6 us (5%)
  local copies, waits for them, and re-layouts  9.34 us (3%)
    reduce_scatter x2, waiting for transfers between devices, local(): lax.psum_scatter(operands[1], 'ra', scatter_dimension=0, tiled=True)  63.6 us
    psum x2, waiting for transfers between devices, local(): lax.psum(terms.astype(jnp.bfloat16), 'cb').astype(jnp.float32)  62.8 us
    all_gather x2, blocking collectives, local(): lax.all_gather(hidden, 'ra', axis=0, tiled=True)  34.3 us
    another operation x3, other arithmetic  29.8 us
    psum x2, blocking collectives, local(): total = lax.psum(squares, 'ra')  25.9 us
    reduce_scatter x2, waiting for transfers between devices, local(): lax.psum_scatter(operands[0], 'ra', scatter_dimension=0, tiled=True)  16.6 us
    psum x1, blocking collectives, local(): final_sum = lax.psum(jnp.sum(xvals * xvals, axis=1), 'ra')  11.7 us
    dot_general x2, matrix products, local(): jnp.dot(lax.all_gather(hidden, 'ra', axis=0, tiled=True), down_local, pre...  8.61 us
  transfers between devices with their start and end apart: 6, of which 5 were waited for; matrix products, arithmetic and copies ran while one was open for 10% of the time, Pallas kernels for 0%

commit v1 on v0

v1 whole, which is shorter than its diff:
```python
import functools

import jax
import jax.numpy as jnp
from jax import lax
from jax.experimental import pallas as pl
from jax.experimental.pallas import tpu as pltpu
from jax.sharding import PartitionSpec as P

F32, BF16 = jnp.float32, jnp.bfloat16
MESH = pl.DeviceIdType.MESH
EPS = 1e-06
WIDTH = 256
LAG = 2
PIECES = 4
UP_SLOTS = 6
DOWN_SLOTS = 12


def body(n, layers, dim, share, chunks, stream, wg, wu, wd, gs, us, ds, pg, og, out,
         wub, wdb, usem, dsem, xb, scaled, own, sr, sl, rr, rl, hid, acc, rinv_ref, ss,
         c1s, c1r, c2s, c2r, ssr, rsr, ssl, rsl, shr, shl, rh, sss, rss, cs, cr):
    p = lax.axis_index("ra")
    q = lax.axis_index("cb")
    core = lax.rem(q, 2)
    mate = q + 1 - 2 * core
    xmate = lax.rem(q + 2, 4)
    tokens, cols = stream.shape
    half = tokens // 2
    wide = cols // PIECES
    w = WIDTH
    total = layers * chunks

    def up_copies(t):
        l, c, k = t // chunks, lax.rem(t, chunks), lax.rem(t, UP_SLOTS)
        at = pl.ds(pl.multiple_of(c * w, w), w)
        return (pltpu.make_async_copy(wg.at[l, :, at], wub.at[k, 0], usem.at[k, 0]),
                pltpu.make_async_copy(wu.at[l, :, at], wub.at[k, 1], usem.at[k, 1]))

    def down_copy(t):
        l, c, k = t // chunks, lax.rem(t, chunks), lax.rem(t, DOWN_SLOTS)
        at = pl.ds(pl.multiple_of(c * w, w), w)
        return pltpu.make_async_copy(wd.at[l, at, :], wdb.at[k], dsem.at[k])

    @pl.loop(0, min(UP_SLOTS, total))
    def _(t):
        for copy in up_copies(t):
            copy.start()

    @pl.loop(0, min(DOWN_SLOTS, total))
    def _(t):
        down_copy(t).start()

    barrier = pltpu.get_barrier_semaphore()
    for k in range(1, n):
        pl.semaphore_signal(barrier, inc=1, device_id={"ra": lax.rem(p + k, n)}, device_id_type=MESH)
    pl.semaphore_signal(barrier, inc=1, device_id={"cb": mate}, device_id_type=MESH)
    pl.semaphore_signal(barrier, inc=1, device_id={"cb": xmate}, device_id_type=MESH)
    pl.semaphore_wait(barrier, n + 1)

    def remote(src, dst, send, recv, **where):
        return pltpu.make_async_remote_copy(src_ref=src, dst_ref=dst, send_sem=send, recv_sem=recv,
                                            device_id=where, device_id_type=MESH)

    right, left = jnp.minimum(p + 1, n - 1), jnp.maximum(p - 1, 0)

    def right_sum(t, c, d):
        return remote(sr.at[t, d], rr.at[t, d], ssr.at[c, d], rsr.at[c, d], ra=right)

    def left_sum(t, c, d):
        return remote(sl.at[t, d], rl.at[t, d], ssl.at[c, d], rsl.at[c, d], ra=left)

    def right_hid(t, c, o):
        return remote(hid.at[t, o], hid.at[t, o], shr.at[c, o], rh.at[c, o], ra=right)

    def left_hid(t, c, o):
        return remote(hid.at[t, o], hid.at[t, o], shl.at[c, o], rh.at[c, o], ra=left)

    def square_copy(l, k, src):
        return remote(ss.at[l, src], ss.at[l, src], sss.at[l, k], rss.at[l, src], ra=lax.rem(p + k, n))

    def send_squares(l):
        col = jnp.zeros((tokens, 1), F32)
        for j in range(PIECES):
            x = xb[l, j].astype(F32)
            col += jnp.sum(x * x, axis=1, keepdims=True)
        eye = (lax.broadcasted_iota(jnp.int32, (tokens, tokens), 0)
               == lax.broadcasted_iota(jnp.int32, (tokens, tokens), 1))
        row = jnp.sum(jnp.where(eye, col, 0.0), axis=0, keepdims=True)
        ss[l, p] = jnp.broadcast_to(row, (8, tokens))
        for k in range(1, n):
            square_copy(l, k, p).start()

    def take_rinv(l, first, rows):
        for k in range(1, n):
            src = lax.rem(p + k, n)
            square_copy(l, k, src).wait_recv()
        row = ss[l, 0][0:1]
        for src in range(1, n):
            row = row + ss[l, src][0:1]
        pick = (lax.broadcasted_iota(jnp.int32, (rows, tokens), 0) + first
                == lax.broadcasted_iota(jnp.int32, (rows, tokens), 1))
        col = jnp.sum(jnp.where(pick, row, 0.0), axis=1, keepdims=True)
        return lax.rsqrt(col / dim + EPS)

    def end_squares(l):
        for k in range(1, n):
            square_copy(l, k, p).wait_send()

    for j in range(PIECES):
        xb[0, j] = stream[:, j * wide:(j + 1) * wide]

    def layer(l):
        send_squares(l)
        for j in range(PIECES):
            at = pl.ds(j * wide, wide)
            scaled[:, at] = (xb[l, j].astype(F32) * pg[pl.ds(l, 1), at]).astype(BF16)
        acc[...] = jnp.zeros_like(acc)

        def products(c):
            t = l * chunks + c
            k = lax.rem(t, UP_SLOTS)
            for copy in up_copies(t):
                copy.wait()
            for side in range(2):
                part = jnp.dot(scaled[...], wub[k, side].astype(BF16), preferred_element_type=F32)
                for d in range(n):
                    own[c, d, :, side * w:(side + 1) * w] = part[d * share:(d + 1) * share]

            @pl.when(t + UP_SLOTS < total)
            def _():
                for copy in up_copies(t + UP_SLOTS):
                    copy.start()

            @pl.when(p == 0)
            def _():
                for d in range(n - 1, 0, -1):
                    sr[t, d] = own[c, d].astype(BF16)
                    right_sum(t, c, d).start()

            @pl.when(p == n - 1)
            def _():
                for d in range(n - 1):
                    sl[t, d] = own[c, d].astype(BF16)
                    left_sum(t, c, d).start()

        def hop(c, h):
            t = l * chunks + c

            @pl.when(p == h)
            def _():
                for d in range(n - 1, h, -1):
                    right_sum(t, c, d).wait_recv()
                    sr[t, d] = (own[c, d] + rr[t, d].astype(F32)).astype(BF16)
                    right_sum(t, c, d).start()

            @pl.when(p == n - 1 - h)
            def _():
                for d in range(n - 1 - h):
                    left_sum(t, c, d).wait_recv()
                    sl[t, d] = (own[c, d] + rl[t, d].astype(F32)).astype(BF16)
                    left_sum(t, c, d).start()

        def finish(c):
            t = l * chunks + c

            @pl.when(c == 0)
            def _():
                rinv_ref[...] = jnp.broadcast_to(take_rinv(l, p * share, share), rinv_ref.shape)

            @pl.when(p > 0)
            def _():
                right_sum(t, c, p).wait_recv()
                own[c, p] += rr[t, p].astype(F32)

            @pl.when(p < n - 1)
            def _():
                left_sum(t, c, p).wait_recv()
                own[c, p] += rl[t, p].astype(F32)

            at = pl.ds(pl.multiple_of(c * w, w), w)
            rinv = rinv_ref[:, 0:1]
            gate = own[c, p, :, 0:w] * rinv * gs[pl.ds(l, 1), at]
            upper = own[c, p, :, w:2 * w] * rinv * us[pl.ds(l, 1), at]
            hid[t, p] = (gate / (1.0 + jnp.exp(-gate)) * upper).astype(BF16)

            @pl.when(p < n - 1)
            def _():
                right_hid(t, c, p).start()

            @pl.when(p > 0)
            def _():
                left_hid(t, c, p).start()

        def pass_on(c, k):
            t = l * chunks + c

            @pl.when(p >= k)
            def _():
                right_hid(t, c, p - k).wait_recv()

                @pl.when(p < n - 1)
                def _():
                    right_hid(t, c, p - k).start()

            @pl.when(p + k <= n - 1)
            def _():
                left_hid(t, c, p + k).wait_recv()

                @pl.when(p > 0)
                def _():
                    left_hid(t, c, p + k).start()

        def down(c):
            t = l * chunks + c
            k = lax.rem(t, DOWN_SLOTS)
            down_copy(t).wait()
            rows = jnp.concatenate([hid[t, d] for d in range(n)], axis=0)
            acc[...] += jnp.dot(rows, wdb[k].astype(BF16), preferred_element_type=F32)

            @pl.when(t + DOWN_SLOTS < total)
            def _():
                down_copy(t + DOWN_SLOTS).start()

        stages = [products]
        stages += [functools.partial(hop, h=h) for h in range(1, n - 1)]
        stages += [finish]
        stages += [functools.partial(pass_on, k=k) for k in range(1, n)]

        @pl.loop(0, chunks + LAG * (len(stages) - 1))
        def _(i):
            for place, stage in enumerate(stages):
                c = i - LAG * place

                @pl.when((c >= 0) & (c < chunks))
                def _(stage=stage, c=c):
                    stage(c)
                    if place == len(stages) - 1:
                        down(c)

        def core_copy(j):
            return remote(c1s.at[l, j], c1r.at[l, j], cs.at[0, l, j], cr.at[0, l, j], cb=mate)

        def chip_copy(j):
            return remote(c2s.at[l, j], c2r.at[l, j], cs.at[1, l, j], cr.at[1, l, j], cb=xmate)

        mine = pl.ds(pl.multiple_of(core * half, half), half)
        other = pl.ds(pl.multiple_of((1 - core) * half, half), half)

        def back_copy(j, rows):
            return remote(xb.at[l + 1, j, rows], xb.at[l + 1, j, rows],
                          cs.at[2, l, j], cr.at[2, l, j], cb=mate)

        for j in range(PIECES):
            c1s[l, j] = acc[other, j * wide:(j + 1) * wide].astype(BF16)
            core_copy(j).start()
        for j in range(PIECES):
            core_copy(j).wait_recv()
            c2s[l, j] = (acc[mine, j * wide:(j + 1) * wide] + c1r[l, j].astype(F32)).astype(BF16)
            chip_copy(j).start()

        @pl.loop(0, chunks)
        def _(c):
            t = l * chunks + c
            for d in range(n):
                @pl.when(p < d)
                def _():
                    right_sum(t, c, d).wait_send()

                @pl.when(p > d)
                def _():
                    left_sum(t, c, d).wait_send()

                @pl.when((d <= p) & (p < n - 1))
                def _():
                    right_hid(t, c, d).wait_send()

                @pl.when((d >= p) & (p > 0))
                def _():
                    left_hid(t, c, d).wait_send()
        end_squares(l)

        for j in range(PIECES):
            chip_copy(j).wait_recv()
            at = pl.ds(j * wide, wide)
            branch = (c2s[l, j].astype(F32) + c2r[l, j].astype(F32)) * ds[pl.ds(l, 1), at]
            xb[l + 1, j, mine] = (0.5 * xb[l, j, mine].astype(F32) + branch).astype(BF16)
            back_copy(j, mine).start()
        for j in range(PIECES):
            back_copy(j, other).wait_recv()
            core_copy(j).wait_send()
            chip_copy(j).wait_send()
            back_copy(j, mine).wait_send()

    pl.loop(0, layers)(layer)

    send_squares(layers)
    rinv = take_rinv(layers, 0, tokens)
    for j in range(PIECES):
        at = slice(j * wide, (j + 1) * wide)
        out[:, at] = (xb[layers, j].astype(F32) * rinv * og[0:1, at]).astype(BF16)
    end_squares(layers)


def fused(stream, w_gate, w_up, w_down, gate_scale, up_scale, down_scale, pre_gain, out_gain):
    n = lax.axis_size("ra")
    tokens, cols = stream.shape
    layers, _, units = w_gate.shape
    share, chunks, half, wide = tokens // n, units // WIDTH, tokens // 2, cols // PIECES
    total = layers * chunks
    dma = pltpu.SemaphoreType.DMA
    scratch = [
        pltpu.VMEM((UP_SLOTS, 2, cols, WIDTH), F32),
        pltpu.VMEM((DOWN_SLOTS, WIDTH, cols), F32),
        dma((UP_SLOTS, 2)),
        dma((DOWN_SLOTS,)),
        pltpu.VMEM((layers + 1, PIECES, tokens, wide), BF16),
        pltpu.VMEM((tokens, cols), BF16),
        pltpu.VMEM((chunks, n, share, 2 * WIDTH), F32),
        pltpu.VMEM((total, n, share, 2 * WIDTH), BF16),
        pltpu.VMEM((total, n, share, 2 * WIDTH), BF16),
        pltpu.VMEM((total, n, share, 2 * WIDTH), BF16),
        pltpu.VMEM((total, n, share, 2 * WIDTH), BF16),
        pltpu.VMEM((total, n, share, WIDTH), BF16),
        pltpu.VMEM((tokens, cols), F32),
        pltpu.VMEM((share, 128), F32),
        pltpu.VMEM((layers + 1, n, 8, tokens), F32),
    ]
    scratch += [pltpu.VMEM((layers, PIECES, half, wide), BF16)] * 4
    scratch += [dma((chunks, n))] * 7
    scratch += [dma((layers + 1, n))] * 2
    scratch += [dma((3, layers, PIECES))] * 2
    vmem, hbm = pl.BlockSpec(memory_space=pltpu.VMEM), pl.BlockSpec(memory_space=pl.ANY)
    return pl.pallas_call(
        functools.partial(body, n, layers, cols * n, share, chunks),
        out_shape=jax.ShapeDtypeStruct((tokens, cols), BF16),
        in_specs=[vmem, hbm, hbm, hbm] + [vmem] * 5,
        out_specs=vmem,
        scratch_shapes=scratch,
        compiler_params=pltpu.CompilerParams(
            collective_id=0, has_side_effects=True, vmem_limit_bytes=64 * 1024 * 1024 - 65536
        ),
    )(stream, w_gate, w_up, w_down, gate_scale, up_scale, down_scale, pre_gain, out_gain[None])


def plain(stream, w_gate, w_up, w_down, gate_scale, up_scale, down_scale, pre_gain, out_gain):
    current = stream
    tokens = stream.shape[0]
    dim = stream.shape[1] * lax.axis_size("ra")
    share = tokens // lax.axis_size("ra")
    for layer in range(w_gate.shape[0]):
        xvals = current.astype(F32)
        squares = jnp.sum(xvals * xvals, axis=1)
        scaled = (xvals * pre_gain[layer]).astype(BF16)
        gate_part = jnp.dot(scaled, w_gate[layer].astype(BF16), preferred_element_type=F32)
        up_part = jnp.dot(scaled, w_up[layer].astype(BF16), preferred_element_type=F32)
        down_local = w_down[layer].astype(BF16)
        total = lax.psum(squares, "ra")
        summed = (
            lax.psum_scatter(gate_part, "ra", scatter_dimension=0, tiled=True),
            lax.psum_scatter(up_part, "ra", scatter_dimension=0, tiled=True),
        )
        own_rows = lax.dynamic_slice_in_dim(total, lax.axis_index("ra") * share, share)
        rinv = lax.rsqrt(own_rows / dim + EPS)[:, None]
        gate = summed[0] * rinv * gate_scale[layer]
        upper = summed[1] * rinv * up_scale[layer]
        hidden = (jax.nn.silu(gate) * upper).astype(BF16)
        terms = jnp.dot(
            lax.all_gather(hidden, "ra", axis=0, tiled=True), down_local, preferred_element_type=F32
        )
        branch = lax.psum(terms.astype(BF16), "cb").astype(F32) * down_scale[layer]
        current = (0.5 * xvals + branch).astype(BF16)
    xvals = current.astype(F32)
    final_sum = lax.psum(jnp.sum(xvals * xvals, axis=1), "ra")
    rinv = lax.rsqrt(final_sum / dim + EPS)[:, None]
    return (xvals * rinv * out_gain).astype(BF16)


def local(*args):
    n = lax.axis_size("ra")
    tokens, cols = args[0].shape
    fits = (n >= 2 and tokens % (16 * n) == 0 and tokens == 128 and lax.axis_size("cb") == 4
            and args[1].shape[2] % WIDTH == 0 and cols % (128 * PIECES) == 0)
    return (fused if fits else plain)(*args)


def solution(mesh):
    placed = (
        P("grp", "ra"),
        P(None, "ra", "cb"),
        P(None, "ra", "cb"),
        P(None, "cb", "ra"),
        P(None, "cb"),
        P(None, "cb"),
        P(None, "ra"),
        P(None, "ra"),
        P("ra"),
    )
    return jax.shard_map(
        local, mesh=mesh, in_specs=placed, out_specs=P("grp", "ra"), check_vma=False
    )
```

time: 298 us -> 112 us (0.38)
  waiting for transfers between devices: 143 us -> 0 us
  Pallas kernels: 0 us -> 110 us
  blocking collectives: 71.9 us -> 0 us
  other arithmetic: 36.8 us -> 0 us
  matrix products: 22 us -> 0 us
  between operations: 13.6 us -> 0.01 us
  local copies, waits for them, and re-layouts: 9.34 us -> 1.67 us
    pallas_call x0 -> x1, Pallas kernels: none -> 110 us  [fused(): pl.pallas_call(functools.partial(body, n, layers, cols * n, share, chunks...]
    reduce_scatter x4 -> x0, waiting for transfers between devices: 80.2 us -> none  [the longest x2 63.6 us: local(): lax.psum_scatter(operands[1], 'ra', scatter_dimension=0, tiled=True)]
    psum x2 -> x0, waiting for transfers between devices: 62.8 us -> none  [local(): lax.psum(terms.astype(jnp.bfloat16), 'cb').astype(jnp.float32)]
    psum x3 -> x0, blocking collectives: 37.6 us -> none  [the longest x2 25.9 us: local(): total = lax.psum(squares, 'ra')]
    all_gather x2 -> x0, blocking collectives: 34.3 us -> none  [local(): lax.all_gather(hidden, 'ra', axis=0, tiled=True)]
    another operation x3 -> x0, other arithmetic: 29.8 us -> none
    dot_general x6 -> x0, matrix products: 22 us -> none  [the longest x2 8.61 us: local(): jnp.dot(lax.all_gather(hidden, 'ra', axis=0, tiled=True), down_local, pre...]
    unnamed x14 -> x1, local copies, waits for them, and re-layouts: 8.44 us -> 1.67 us
  transfers between devices with their start and end apart: 6 -> 0, of which waited for: 5 -> 0; matrix products, arithmetic and copies ran while one was open for 10% -> 0% of each run, Pallas kernels for 0% -> 0%
where the time goes in v1:
time: 112 us
  Pallas kernels  110 us (98%)
  local copies, waits for them, and re-layouts  1.67 us (1%)
    pallas_call x1, Pallas kernels, fused(): pl.pallas_call(functools.partial(body, n, layers, cols * n, share, chunks...  110 us

profile of v1, /device:TPU:0, one launch (start us, length us, event | category | flops | bytes accessed | tf_op | source)
XLA Modules:
  0.0 112.0 jit_solution(11984914948954570967)
XLA Ops:
  0.0 110.3 %shard_map.91 = bf16[128,1024]{1,0:T(8,128)(2,1)} custom-call(bf16[128,1024]{1,0:T(8,128)(2,1)} %stream.1, f32[2,1024,2816]{2,1,0:T(8,128)} %wg.1, f32[2,1024,2816]{2,1,0:T(8,128)} %wu.1, f32[2,2816,1024]{2,1,0:T(8,128)} %wd.1, f32[2,2816]{1,0:T(2,128)} %gs.1, f32[2,2816]{1,0:T(2,128)} %us.1, f32[2,1024]{1,0:T(2,128)} %ds.1, f32[2,1024]{1,0:T(2,128)} %pg.1, ...), custom_call_target="tpu_custom_call" | custom-call | tf_op jit(solution)/shard_map/pallas_call | solution.py:334
  110.3 1.7 %copy.11 = bf16[128,1024]{1,0:T(8,128)(2,1)} copy(bf16[128,1024]{1,0:T(8,128)(2,1)} %shard_map.91) | data formatting | bytes 524288

commit v2 on v1

--- a/solution.py
+++ b/solution.py
@@ -11,15 +11,16 @@
 MESH = pl.DeviceIdType.MESH
 EPS = 1e-06
 WIDTH = 256
-LAG = 2
-PIECES = 4
+LAG = 3
+PIECES = 2
 UP_SLOTS = 6
+FIRST = 2
 DOWN_SLOTS = 12
 
 
 def body(n, layers, dim, share, chunks, stream, wg, wu, wd, gs, us, ds, pg, og, out,
-         wub, wdb, usem, dsem, xb, scaled, own, sr, sl, rr, rl, hid, acc, rinv_ref, ss,
-         c1s, c1r, c2s, c2r, ssr, rsr, ssl, rsl, shr, shl, rh, sss, rss, cs, cr):
+         wub, wdb, usem, dsem, xb, scaled, own, sums, got, hid, acc, rinv_ref, scales, ss,
+         c1s, c1r, c2s, c2r, ssum, rsum, shid, rhid, sss, rss, cs, cr):
     p = lax.axis_index("ra")
     q = lax.axis_index("cb")
     core = lax.rem(q, 2)
@@ -42,14 +43,9 @@
         at = pl.ds(pl.multiple_of(c * w, w), w)
         return pltpu.make_async_copy(wd.at[l, at, :], wdb.at[k], dsem.at[k])
 
-    @pl.loop(0, min(UP_SLOTS, total))
-    def _(t):
+    for t in range(FIRST):
         for copy in up_copies(t):
             copy.start()
-
-    @pl.loop(0, min(DOWN_SLOTS, total))
-    def _(t):
-        down_copy(t).start()
 
     barrier = pltpu.get_barrier_semaphore()
     for k in range(1, n):
@@ -64,17 +60,11 @@
 
     right, left = jnp.minimum(p + 1, n - 1), jnp.maximum(p - 1, 0)
 
-    def right_sum(t, c, d):
-        return remote(sr.at[t, d], rr.at[t, d], ssr.at[c, d], rsr.at[c, d], ra=right)
-
-    def left_sum(t, c, d):
-        return remote(sl.at[t, d], rl.at[t, d], ssl.at[c, d], rsl.at[c, d], ra=left)
-
-    def right_hid(t, c, o):
-        return remote(hid.at[t, o], hid.at[t, o], shr.at[c, o], rh.at[c, o], ra=right)
-
-    def left_hid(t, c, o):
-        return remote(hid.at[t, o], hid.at[t, o], shl.at[c, o], rh.at[c, o], ra=left)
+    def sum_copy(t, c, e):
+        return remote(sums.at[t, e], got.at[t, e], ssum.at[c, e], rsum.at[c, e], ra=right if e else left)
+
+    def hid_copy(t, c, e):
+        return remote(hid.at[t, e], hid.at[t, e], shid.at[c, e], rhid.at[c, e], ra=left if e else right)
 
     def square_copy(l, k, src):
         return remote(ss.at[l, src], ss.at[l, src], sss.at[l, k], rss.at[l, src], ra=lax.rem(p + k, n))
@@ -107,6 +97,10 @@
         for k in range(1, n):
             square_copy(l, k, p).wait_send()
 
+    for t in range(total):
+        row, at = slice(t // chunks, t // chunks + 1), slice(t % chunks * w, (t % chunks + 1) * w)
+        scales[t, 0:1] = gs[row, at]
+        scales[t, 1:2] = us[row, at]
     for j in range(PIECES):
         xb[0, j] = stream[:, j * wide:(j + 1) * wide]
 
@@ -122,100 +116,78 @@
             k = lax.rem(t, UP_SLOTS)
             for copy in up_copies(t):
                 copy.wait()
+
+            @pl.when(t == 0)
+            def _():
+                @pl.loop(FIRST, min(UP_SLOTS, total))
+                def _(later):
+                    for copy in up_copies(later):
+                        copy.start()
+
+                @pl.loop(0, min(DOWN_SLOTS, total))
+                def _(later):
+                    down_copy(later).start()
+
             for side in range(2):
                 part = jnp.dot(scaled[...], wub[k, side].astype(BF16), preferred_element_type=F32)
-                for d in range(n):
-                    own[c, d, :, side * w:(side + 1) * w] = part[d * share:(d + 1) * share]
+                for e in range(2):
+                    own[c, e, :, side * w:(side + 1) * w] = part[e * share:(e + 1) * share]
 
             @pl.when(t + UP_SLOTS < total)
             def _():
                 for copy in up_copies(t + UP_SLOTS):
                     copy.start()
 
-            @pl.when(p == 0)
-            def _():
-                for d in range(n - 1, 0, -1):
-                    sr[t, d] = own[c, d].astype(BF16)
-                    right_sum(t, c, d).start()
-
-            @pl.when(p == n - 1)
-            def _():
-                for d in range(n - 1):
-                    sl[t, d] = own[c, d].astype(BF16)
-                    left_sum(t, c, d).start()
+            for e in range(2):
+                @pl.when(p == (0 if e else n - 1))
+                def _():
+                    sums[t, e] = own[c, e].astype(BF16)
+                    sum_copy(t, c, e).start()
 
         def hop(c, h):
             t = l * chunks + c
-
-            @pl.when(p == h)
-            def _():
-                for d in range(n - 1, h, -1):
-                    right_sum(t, c, d).wait_recv()
-                    sr[t, d] = (own[c, d] + rr[t, d].astype(F32)).astype(BF16)
-                    right_sum(t, c, d).start()
-
-            @pl.when(p == n - 1 - h)
-            def _():
-                for d in range(n - 1 - h):
-                    left_sum(t, c, d).wait_recv()
-                    sl[t, d] = (own[c, d] + rl[t, d].astype(F32)).astype(BF16)
-                    left_sum(t, c, d).start()
+            for e in range(2):
+                @pl.when(p == (h if e else n - 1 - h))
+                def _():
+                    sum_copy(t, c, e).wait_recv()
+                    sums[t, e] = (own[c, e] + got[t, e].astype(F32)).astype(BF16)
+                    sum_copy(t, c, e).start()
 
         def finish(c):
-            t = l * chunks + c
-
             @pl.when(c == 0)
             def _():
-                rinv_ref[...] = jnp.broadcast_to(take_rinv(l, p * share, share), rinv_ref.shape)
-
-            @pl.when(p > 0)
-            def _():
-                right_sum(t, c, p).wait_recv()
-                own[c, p] += rr[t, p].astype(F32)
-
-            @pl.when(p < n - 1)
-            def _():
-                left_sum(t, c, p).wait_recv()
-                own[c, p] += rl[t, p].astype(F32)
-
-            at = pl.ds(pl.multiple_of(c * w, w), w)
+                first = jnp.where(p == 0, 0, share)
+                rinv_ref[...] = jnp.broadcast_to(take_rinv(l, first, share), rinv_ref.shape)
+
+            for e in range(2):
+                @pl.when(p == (n - 1 if e else 0))
+                def _():
+                    activate(c, e)
+
+        def activate(c, e):
+            t = l * chunks + c
+            sum_copy(t, c, e).wait_recv()
+            both = own[c, e] + got[t, e].astype(F32)
             rinv = rinv_ref[:, 0:1]
-            gate = own[c, p, :, 0:w] * rinv * gs[pl.ds(l, 1), at]
-            upper = own[c, p, :, w:2 * w] * rinv * us[pl.ds(l, 1), at]
-            hid[t, p] = (gate / (1.0 + jnp.exp(-gate)) * upper).astype(BF16)
-
-            @pl.when(p < n - 1)
-            def _():
-                right_hid(t, c, p).start()
-
-            @pl.when(p > 0)
-            def _():
-                left_hid(t, c, p).start()
+            gate = both[:, 0:w] * rinv * scales[t, 0:1]
+            upper = both[:, w:2 * w] * rinv * scales[t, 1:2]
+            hid[t, e] = (gate / (1.0 + jnp.exp(-gate)) * upper).astype(BF16)
+            hid_copy(t, c, e).start()
 
         def pass_on(c, k):
             t = l * chunks + c
-
-            @pl.when(p >= k)
-            def _():
-                right_hid(t, c, p - k).wait_recv()
-
-                @pl.when(p < n - 1)
-                def _():
-                    right_hid(t, c, p - k).start()
-
-            @pl.when(p + k <= n - 1)
-            def _():
-                left_hid(t, c, p + k).wait_recv()
-
-                @pl.when(p > 0)
-                def _():
-                    left_hid(t, c, p + k).start()
+            for e in range(2):
+                @pl.when(p == (n - 1 - k if e else k))
+                def _():
+                    hid_copy(t, c, e).wait_recv()
+                    if k < n - 1:
+                        hid_copy(t, c, e).start()
 
         def down(c):
             t = l * chunks + c
             k = lax.rem(t, DOWN_SLOTS)
             down_copy(t).wait()
-            rows = jnp.concatenate([hid[t, d] for d in range(n)], axis=0)
+            rows = jnp.concatenate([hid[t, 0], hid[t, 1]], axis=0)
             acc[...] += jnp.dot(rows, wdb[k].astype(BF16), preferred_element_type=F32)
 
             @pl.when(t + DOWN_SLOTS < total)
@@ -262,22 +234,14 @@
         @pl.loop(0, chunks)
         def _(c):
             t = l * chunks + c
-            for d in range(n):
-                @pl.when(p < d)
-                def _():
-                    right_sum(t, c, d).wait_send()
-
-                @pl.when(p > d)
-                def _():
-                    left_sum(t, c, d).wait_send()
-
-                @pl.when((d <= p) & (p < n - 1))
-                def _():
-                    right_hid(t, c, d).wait_send()
-
-                @pl.when((d >= p) & (p > 0))
-                def _():
-                    left_hid(t, c, d).wait_send()
+            for e in range(2):
+                @pl.when(p != (n - 1 if e else 0))
+                def _():
+                    sum_copy(t, c, e).wait_send()
+
+                @pl.when(p != (0 if e else n - 1))
+                def _():
+                    hid_copy(t, c, e).wait_send()
         end_squares(l)
 
         for j in range(PIECES):
@@ -306,7 +270,7 @@
     n = lax.axis_size("ra")
     tokens, cols = stream.shape
     layers, _, units = w_gate.shape
-    share, chunks, half, wide = tokens // n, units // WIDTH, tokens // 2, cols // PIECES
+    share, chunks, half, wide = tokens // 2, units // WIDTH, tokens // 2, cols // PIECES
     total = layers * chunks
     dma = pltpu.SemaphoreType.DMA
     scratch = [
@@ -316,18 +280,17 @@
         dma((DOWN_SLOTS,)),
         pltpu.VMEM((layers + 1, PIECES, tokens, wide), BF16),
         pltpu.VMEM((tokens, cols), BF16),
-        pltpu.VMEM((chunks, n, share, 2 * WIDTH), F32),
-        pltpu.VMEM((total, n, share, 2 * WIDTH), BF16),
-        pltpu.VMEM((total, n, share, 2 * WIDTH), BF16),
-        pltpu.VMEM((total, n, share, 2 * WIDTH), BF16),
-        pltpu.VMEM((total, n, share, 2 * WIDTH), BF16),
-        pltpu.VMEM((total, n, share, WIDTH), BF16),
+        pltpu.VMEM((chunks, 2, share, 2 * WIDTH), F32),
+        pltpu.VMEM((total, 2, share, 2 * WIDTH), BF16),
+        pltpu.VMEM((total, 2, share, 2 * WIDTH), BF16),
+        pltpu.VMEM((total, 2, share, WIDTH), BF16),
         pltpu.VMEM((tokens, cols), F32),
         pltpu.VMEM((share, 128), F32),
+        pltpu.VMEM((total, 8, WIDTH), F32),
         pltpu.VMEM((layers + 1, n, 8, tokens), F32),
     ]
     scratch += [pltpu.VMEM((layers, PIECES, half, wide), BF16)] * 4
-    scratch += [dma((chunks, n))] * 7
+    scratch += [dma((chunks, 2))] * 4
     scratch += [dma((layers + 1, n))] * 2
     scratch += [dma((3, layers, PIECES))] * 2
     vmem, hbm = pl.BlockSpec(memory_space=pltpu.VMEM), pl.BlockSpec(memory_space=pl.ANY)
@@ -379,7 +342,7 @@
 def local(*args):
     n = lax.axis_size("ra")
     tokens, cols = args[0].shape
-    fits = (n >= 2 and tokens % (16 * n) == 0 and tokens == 128 and lax.axis_size("cb") == 4
+    fits = (n >= 2 and tokens == 128 and n <= 8 and lax.axis_size("cb") == 4
             and args[1].shape[2] % WIDTH == 0 and cols % (128 * PIECES) == 0)
     return (fused if fits else plain)(*args)
 

time: 112 us -> 100 us (0.89)
  Pallas kernels: 110 us -> 98.2 us
    pallas_call x1, Pallas kernels: 110 us -> 98.2 us  [fused(): pl.pallas_call(functools.partial(body, n, layers, cols * n, share, chunks...]
where the time goes in v2:
time: 100 us; the launch traced here: 99.9 us
  Pallas kernels  98.2 us (98%)
  local copies, waits for them, and re-layouts  1.67 us (2%)
    pallas_call x1, Pallas kernels, fused(): pl.pallas_call(functools.partial(body, n, layers, cols * n, share, chunks...  98.2 us

profile of v2, /device:TPU:0, one launch (start us, length us, event | category | flops | bytes accessed | tf_op | source)
XLA Modules:
  0.0 99.9 jit_solution(13949949632549488420)
XLA Ops:
  0.0 98.2 %shard_map.91 = bf16[128,1024]{1,0:T(8,128)(2,1)} custom-call(bf16[128,1024]{1,0:T(8,128)(2,1)} %stream.1, f32[2,1024,2816]{2,1,0:T(8,128)} %wg.1, f32[2,1024,2816]{2,1,0:T(8,128)} %wu.1, f32[2,2816,1024]{2,1,0:T(8,128)} %wd.1, f32[2,2816]{1,0:T(2,128)} %gs.1, f32[2,2816]{1,0:T(2,128)} %us.1, f32[2,1024]{1,0:T(2,128)} %ds.1, f32[2,1024]{1,0:T(2,128)} %pg.1, ...), custom_call_target="tpu_custom_call" | custom-call | tf_op jit(solution)/shard_map/pallas_call | solution.py:297
  98.2 1.7 %copy.11 = bf16[128,1024]{1,0:T(8,128)(2,1)} copy(bf16[128,1024]{1,0:T(8,128)(2,1)} %shard_map.91) | data formatting | bytes 524288
